TPU v7x, 32 devices: a whole 2x2x4 slice. The times are simulated.
32 devices in a mesh: sp: 4 (over z), fs: 4 (over y, x), tp: 2 (over core).
Axes of the slice: x: 2, y: 2, z: 4, core: 2. Of those that a mesh axis runs over, the one named last changes fastest.
Arguments:
- queries: bfloat16 [4, 1024, 512], P('fs', 'sp', 'tp'), may hold values from -60 to 60
- keys: bfloat16 [4, 1024, 256], P('fs', 'sp', 'tp'), may hold values from -4.5 to 4.5
- values: bfloat16 [4, 1024, 256], P('fs', 'sp', 'tp'), may hold values from -6 to 6
- forget_cache: float32 [4, 1024, 8], P('fs', 'sp', 'tp'), may hold values from -128 to 0, as said below
- fox_gain: float32 [512], P('tp'), may hold values from 0.1 to 1.9
- receptance: bfloat16 [4, 1024, 512], P('fs', 'sp', 'tp'), may hold values from -6 to 6
- lin_keys: bfloat16 [4, 1024, 512], P('fs', 'sp', 'tp'), may hold values from -6 to 6
- lin_values: bfloat16 [4, 1024, 512], P('fs', 'sp', 'tp'), may hold values from -6 to 6
- learn_logit: bfloat16 [4, 1024, 512], P('fs', 'sp', 'tp'), may hold values from -12 to 4
- decay_log: float32 [4, 1024, 512], P('fs', 'sp', 'tp'), may hold values from -16 to 0
- lin_gain: float32 [512], P('tp'), may hold values from 0.1 to 1.9
- out_fox_weight: bfloat16 [512, 2048], P('tp', 'fs'), may hold values from -0.1875 to 0.1875
- out_lin_weight: bfloat16 [512, 2048], P('tp', 'fs'), may hold values from -0.1875 to 0.1875
Outputs:
- mixed: bfloat16 [4, 1024, 2048], P('fs', ('sp', 'tp'))
Inputs may be any that keep to these rules, and one draw needn't show every extreme that they name: `forget_cache`: Non-increasing along the positions of each sequence and head.
All inputs are finite; a program needn't handle non-finite values.
Results may differ from a plain program's by a relative error of at most 0.017.
Values may be sent and summed in bfloat16 or wider, within the bound.
A program may use at most 64 MiB of HBM per device.

v0:
```python
import math
import jax
import jax.numpy as jnp
from jax import lax
from jax.sharding import PartitionSpec as P

HEAD = 64
SPAN = 64
HIGHEST = lax.Precision.HIGHEST
NORM_EPS = 1e-06


def carried_in(shard, axis, join, neutral):
    place = lax.axis_index(axis)
    gathered = jax.tree.map(
        lambda a, kind: lax.all_gather(a.astype(kind), axis), shard, (jnp.bfloat16, jnp.bfloat16)
    )
    state = jax.tree.map(lambda a, e: jnp.zeros_like(a) + jnp.asarray(e, a.dtype), shard, neutral)

    def one(lap, state):
        return join(
            state,
            jax.tree.map(
                lambda a, own: lax.dynamic_index_in_dim(a, lap, 0, False).astype(own.dtype),
                gathered,
                shard,
            ),
        )

    return lax.fori_loop(0, place, one, state)


def round_half(tensor):
    return lax.optimization_barrier(tensor.astype(jnp.bfloat16)).astype(jnp.float32)


def forget_attention(query_rows, key_rows, value_rows, forget_rows, fox_gain):
    row_count = query_rows.shape[0]
    head_count = query_rows.shape[1] // HEAD
    kv_count = key_rows.shape[1] // HEAD
    group_size = head_count // kv_count
    score_scale = HEAD ** (-0.5)
    own_first = lax.axis_index("sp") * row_count
    forget_all = lax.all_gather(forget_rows, "sp", axis=0, tiled=True)
    forget_own = forget_rows.reshape(row_count, kv_count, group_size)
    query_heads = query_rows.reshape(row_count, kv_count, group_size, HEAD)
    query_pos = own_first + jnp.arange(row_count, dtype=jnp.int32)
    start_state = (
        jnp.full((row_count, kv_count, group_size), -1e30, jnp.float32),
        jnp.zeros((row_count, kv_count, group_size), jnp.float32),
        jnp.zeros((row_count, kv_count, group_size, HEAD), jnp.float32),
    )
    key_piece = lax.all_gather(key_rows, "sp", axis=0, tiled=True)
    value_piece = lax.all_gather(value_rows, "sp", axis=0, tiled=True)
    piece_rows = key_piece.shape[0]
    block_rows = math.gcd(piece_rows, 512)

    def attend(state):

        def one_block(block_index, inner):
            running_max, totals, weighted = inner
            local_first = (block_index * block_rows).astype(jnp.int32)
            key_block = lax.dynamic_slice_in_dim(key_piece, local_first, block_rows, 0).reshape(
                block_rows, kv_count, HEAD
            )
            value_block = lax.dynamic_slice_in_dim(value_piece, local_first, block_rows, 0).reshape(
                block_rows, kv_count, HEAD
            )
            forget_block = lax.dynamic_slice_in_dim(forget_all, local_first, block_rows, 0).reshape(
                block_rows, kv_count, group_size
            )
            key_pos = local_first + jnp.arange(block_rows, dtype=jnp.int32)
            allowed = (key_pos[None, :] <= query_pos[:, None])[:, None, None, :]
            scores = jnp.einsum(
                "tkgd,skd->tkgs", query_heads, key_block, preferred_element_type=jnp.float32
            )
            scores = (
                scores * score_scale
                + forget_own[..., None]
                - jnp.transpose(forget_block, (1, 2, 0))[None]
            )
            scores = jnp.where(allowed, scores, -1e30)
            new_max = jnp.maximum(running_max, jnp.max(scores, axis=-1))
            rescale = jnp.exp(running_max - new_max)
            weights = jnp.where(allowed, jnp.exp(scores - new_max[..., None]), 0.0)
            totals = totals * rescale + jnp.sum(weights, axis=-1)
            update = jnp.einsum(
                "tkgs,skd->tkgd",
                weights.astype(jnp.bfloat16),
                value_block,
                preferred_element_type=jnp.float32,
            )
            weighted = weighted * rescale[..., None] + update
            return (new_max, totals, weighted)

        return lax.fori_loop(0, piece_rows // block_rows, one_block, state)

    def keep_state(running_state):
        return running_state

    running_max, totals, weighted = lax.cond(
        jnp.int32(0) < own_first + row_count, attend, keep_state, start_state
    )
    attended = (weighted / totals[..., None]).reshape(row_count, head_count, HEAD)
    normed = attended * lax.rsqrt(jnp.mean(attended * attended, axis=-1, keepdims=True) + NORM_EPS)
    return (
        (normed * fox_gain.reshape(head_count, HEAD))
        .reshape(row_count, head_count * HEAD)
        .astype(jnp.bfloat16)
    )


def product(left, right, form):
    return jnp.einsum(form, left, right, precision=HIGHEST)


def delta_attention(recept_rows, key_rows, value_rows, learn_rows, decay_rows, lin_gain):
    row_count = recept_rows.shape[0]
    head_count = recept_rows.shape[1] // HEAD
    span_count = row_count // SPAN

    def arrange(tensor):
        return jnp.transpose(
            tensor.astype(jnp.float32).reshape(span_count, SPAN, head_count, HEAD), (0, 2, 1, 3)
        )

    recept = arrange(recept_rows)
    key_float = arrange(key_rows)
    value_float = arrange(value_rows)
    learn_rate = jax.nn.sigmoid(arrange(learn_rows))
    unit_keys = key_float * lax.rsqrt(
        jnp.sum(key_float * key_float, axis=-1, keepdims=True) + NORM_EPS
    )
    log_decay = -jnp.exp(arrange(decay_rows))
    strict_lower = jnp.tril(jnp.ones((SPAN, SPAN), jnp.float32), -1)
    with_diagonal = jnp.tril(jnp.ones((SPAN, SPAN), jnp.float32))
    identity_head = jnp.broadcast_to(jnp.eye(HEAD, dtype=jnp.float32), (head_count, HEAD, HEAD))
    identity_span = jnp.broadcast_to(jnp.eye(SPAN, dtype=jnp.float32), (head_count, SPAN, SPAN))
    zero_state = jnp.zeros((head_count, HEAD, HEAD), jnp.float32)

    def one_span(state, inputs):
        recept_t, key_t, value_t, unit_t, rate_t, fall_t = inputs
        inclusive = jnp.cumsum(fall_t, axis=1)
        grown = jnp.exp(inclusive)
        shrunk = jnp.exp(-inclusive)
        erase_in = -unit_t * jnp.exp(inclusive - fall_t)
        read_in = recept_t * grown
        erase_out = unit_t * rate_t * shrunk
        write_out = key_t * shrunk
        padded_values = jnp.concatenate([value_t, jnp.zeros_like(value_t)], axis=-1)
        mix_erase = product(erase_in, erase_out, "hid,hjd->hij") * strict_lower
        mix_write = product(erase_in, write_out, "hid,hjd->hij") * strict_lower
        read_erase = product(read_in, erase_out, "hid,hjd->hij") * with_diagonal
        read_write = product(read_in, write_out, "hid,hjd->hij") * with_diagonal
        right_side = product(erase_in, state, "hid,hrd->hir") + product(
            mix_write, padded_values, "hij,hjr->hir"
        )
        erased = jax.scipy.linalg.solve_triangular(
            identity_span - mix_erase, right_side, lower=True, unit_diagonal=True
        )
        outputs = (
            product(read_in, state, "hid,hrd->hir")
            + product(read_erase, erased, "hij,hjr->hir")
            + product(read_write, padded_values, "hij,hjr->hir")
        )
        final_grow = grown[:, -1, :]
        state = (
            state * final_grow[:, None, :]
            + product(erased, erase_out * final_grow[:, None, :], "hlr,hld->hrd")
            + product(padded_values, write_out * final_grow[:, None, :], "hlr,hld->hrd")
        )
        return (state, outputs)

    start_state = jnp.concatenate([zero_state, identity_head], axis=1)
    final_state, outputs = lax.scan(
        one_span, start_state, (recept, key_float, value_float, unit_keys, learn_rate, log_decay)
    )
    local_read = outputs[..., :HEAD]
    carried_read = outputs[..., HEAD:]

    def chain(earlier, later):
        return (
            product(earlier[0], later[0], "hij,hjk->hik"),
            product(earlier[1], later[0], "hij,hjk->hik") + later[1],
        )

    entry_map, entry_state = carried_in(
        (final_state[:, HEAD:], final_state[:, :HEAD]), "sp", chain, (identity_head, zero_state)
    )
    readout = local_read + jnp.einsum(
        "hvk,nhtk->nhtv", entry_state, carried_read, precision=HIGHEST
    )
    readout = jnp.transpose(readout, (0, 2, 1, 3)).reshape(row_count, head_count, HEAD)
    centred = readout - jnp.mean(readout, axis=-1, keepdims=True)
    normed = centred * lax.rsqrt(jnp.mean(centred * centred, axis=-1, keepdims=True) + HEAD * 1e-05)
    return (
        (normed * lin_gain.reshape(head_count, HEAD))
        .reshape(row_count, head_count * HEAD)
        .astype(jnp.bfloat16)
    )


def shards(
    queries,
    keys,
    values,
    forget_cache,
    fox_gain,
    receptance,
    lin_keys,
    lin_values,
    learn_logit,
    decay_log,
    lin_gain,
    out_fox_weight,
    out_lin_weight,
):
    fox_out = forget_attention(queries[0], keys[0], values[0], forget_cache[0], fox_gain)
    lin_out = delta_attention(
        receptance[0], lin_keys[0], lin_values[0], learn_logit[0], decay_log[0], lin_gain
    )
    fox_weight, lin_weight = (
        lax.all_gather(out_fox_weight, "fs", axis=1, tiled=True),
        lax.all_gather(out_lin_weight, "fs", axis=1, tiled=True),
    )
    partial_value = jnp.dot(fox_out, fox_weight, preferred_element_type=jnp.float32)
    partial_value = partial_value + jnp.dot(lin_out, lin_weight, preferred_element_type=jnp.float32)
    summed = lax.psum_scatter(
        round_half(partial_value).astype(jnp.bfloat16), "tp", scatter_dimension=0, tiled=True
    )
    return summed[None]


def solution(mesh):
    return jax.shard_map(
        shards,
        mesh=mesh,
        in_specs=(
            P("fs", "sp", "tp"),
            P("fs", "sp", "tp"),
            P("fs", "sp", "tp"),
            P("fs", "sp", "tp"),
            P("tp"),
            P("fs", "sp", "tp"),
            P("fs", "sp", "tp"),
            P("fs", "sp", "tp"),
            P("fs", "sp", "tp"),
            P("fs", "sp", "tp"),
            P("tp"),
            P("tp", "fs"),
            P("tp", "fs"),
        ),
        out_specs=P("fs", ("sp", "tp"), None),
        check_vma=False,
    )
```

profile of v0, /device:TPU:0, one launch (start us, length us, event | category | flops | bytes accessed | tf_op | source)
XLA Modules:
  0.0 230.0 jit_solution(1138776864522754009)
XLA Ops:
  8.1 1.2 reshape.164
  10.2 1.1 reshape.163
  11.3 1.0 neg.24
  13.0 106.6 %while.46 = (s32[]{:T(128)}, f32[4,128,64]{1,2,0:T(8,128)S(1)}, f32[4,4,64,128]{3,2,1,0:T(8,128)}, f32[4,4,64,64]{3,1,2,0:T(4,128)}, f32[4,4,64,64]{3,1,2,0:T(4,...) while((s32[]{:T(128)}, f32[4,128,64]{1,2,0:T(8,128)S(1)}, ...), condition=%wide.region_10.11_spmd.clone.clone, body=%wide.region_8.10_spmd.clone.clone.sunk | while | flops 253308992 | bytes 5993869 | solution.py:175
  13.0 0.9 constant_dynamic-slice_fusion.20
  15.6 19.7 %custom-call.11 = f32[4,1,64,64]{2,3,1,0:T(8,128)S(1)} custom-call(f32[4,1,64,64]{3,2,1,0:T(8,128)S(1)} %fusion.172), custom_call_target="InvertDiagBlocksLowerTriangular" | custom-call | tf_op jit(solution)/shard_map/while/body/eval_jaxpr/jit(_solve_triangular)/vmap()/triangular_solve | solution.py:158
  39.6 0.9 constant_dynamic-slice_fusion.20
  42.2 19.7 %custom-call.11 = f32[4,1,64,64]{2,3,1,0:T(8,128)S(1)} custom-call(f32[4,1,64,64]{3,2,1,0:T(8,128)S(1)} %fusion.172), custom_call_target="InvertDiagBlocksLowerTriangular" | custom-call | tf_op jit(solution)/shard_map/while/body/eval_jaxpr/jit(_solve_triangular)/vmap()/triangular_solve | solution.py:158
  64.5 0.9 fusion.176
  66.3 0.9 constant_dynamic-slice_fusion.20
  68.9 19.7 %custom-call.11 = f32[4,1,64,64]{2,3,1,0:T(8,128)S(1)} custom-call(f32[4,1,64,64]{3,2,1,0:T(8,128)S(1)} %fusion.172), custom_call_target="InvertDiagBlocksLowerTriangular" | custom-call | tf_op jit(solution)/shard_map/while/body/eval_jaxpr/jit(_solve_triangular)/vmap()/triangular_solve | solution.py:158
  91.2 0.9 fusion.176
  92.9 0.9 constant_dynamic-slice_fusion.20
  95.5 19.7 %custom-call.11 = f32[4,1,64,64]{2,3,1,0:T(8,128)S(1)} custom-call(f32[4,1,64,64]{3,2,1,0:T(8,128)S(1)} %fusion.172), custom_call_target="InvertDiagBlocksLowerTriangular" | custom-call | tf_op jit(solution)/shard_map/while/body/eval_jaxpr/jit(_solve_triangular)/vmap()/triangular_solve | solution.py:158
  119.7 15.7 %all-gather.3 = bf16[16,64,64]{2,1,0:T(8,128)(2,1)S(1)} all-gather(bf16[4,64,64]{2,1,0:T(8,128)(2,1)S(1)} %get-tuple-element.533), channel_id=5, replica_groups=mesh['sp'=4,'fs'=4,'tp'=2] {'sp'}, dimensions={0}, use_global_device_ids=true | all-gather | bytes 163840 | tf_op jit(solution)/shard_map/all_gather | solution.py:16
  135.4 14.6 %all-gather.4 = bf16[16,64,64]{2,1,0:T(8,128)(2,1)S(1)} all-gather(bf16[4,64,64]{2,1,0:T(8,128)(2,1)S(1)} %get-tuple-element.532), channel_id=6, replica_groups=mesh['sp'=4,'fs'=4,'tp'=2] {'sp'}, dimensions={0}, use_global_device_ids=true | all-gather | bytes 163840 | tf_op jit(solution)/shard_map/all_gather | solution.py:16
  150.0 1.0 copy-done
  151.4 1.7 fusion.65
  156.0 13.2 %all-gather.1 = f32[1,1024,4]{1,2,0:T(4,128)S(1)} all-gather(f32[1,256,4]{1,2,0:T(4,128)S(1)} %copy-done.10), channel_id=3, replica_groups=mesh['sp'=4,'fs'=4,'tp'=2] {'sp'}, dimensions={1}, use_global_device_ids=true | all-gather | bytes 20480 | tf_op jit(solution)/shard_map/all_gather | solution.py:44
  169.2 14.5 %all-gather = bf16[1,1024,128]{1,2,0:T(8,128)(2,1)S(1)} all-gather(bf16[1,256,128]{1,2,0:T(8,128)(2,1)S(1)} %copy.55), channel_id=2, replica_groups=mesh['sp'=4,'fs'=4,'tp'=2] {'sp'}, dimensions={1}, use_global_device_ids=true | all-gather | bytes 327680 | tf_op jit(solution)/shard_map/all_gather | solution.py:53
  183.7 14.0 %all-gather.2 = bf16[1,1024,128]{1,2,0:T(8,128)(2,1)S(1)} all-gather(bf16[1,256,128]{1,2,0:T(8,128)(2,1)S(1)} %copy.56), channel_id=4, replica_groups=mesh['sp'=4,'fs'=4,'tp'=2] {'sp'}, dimensions={1}, use_global_device_ids=true | all-gather | bytes 327680 | tf_op jit(solution)/shard_map/all_gather | solution.py:54
  197.7 10.5 %conditional.1 = (f32[256,2,2]{0,2,1:T(2,128)}, f32[256,2,2,64]{0,3,2,1:T(8,128)}) conditional(s32[]{:T(128)} %convert_element_type.58, () %tuple.38, (s32[]{:T(128)}, s32[256]{0:T(256)S(1)}, bf16[1,256,256]{2,1,0:T(8,128)(2,1)S(1)}, bf16[1024,128]{0,1:T(8,128)(2,1)S(1)}, f32[1,256,4]{1,2,0:T(4,128)S(1)}, /*index=5*/f32[1024,4]{0,1:T(4,128)S(1)}, ...), branch_computations={%region_0.0_spmd, %region_1.6_spmd} | conditional | flops 140318464 | bytes 8662403 | solution.py:101
  198.5 9.7 %while.44 = (s32[]{:T(128)}, f32[256,2,2]{0,2,1:T(2,128)S(1)}, f32[256,2,2]{0,2,1:T(2,128)}, f32[256,2,2,64]{0,3,2,1:T(8,128)}, s32[256]{0:T(256)S(1)}, /*index=...) while((s32[]{:T(128)}, f32[256,2,2]{0,2,1:T(2,128)S(1)}, ...), condition=%wide.wide.region_5.5_spmd.clone, body=%wide.wide.region_2.4_spmd.clone.sunk | while | flops 140318208 | bytes 8373459 | solution.py:96
  198.7 1.6 fusion.181
  201.4 1.2 fusion.185
  202.8 1.6 fusion.181
  204.8 1.3 fusion.184
  206.1 2.1 fusion.185
  208.2 1.1 multiply_reduce_fusion.2
  209.5 1.7 fusion.67
  211.2 2.7 %fusion.54 = bf16[256,2048]{1,0:T(8,128)(2,1)} fusion(f32[256,2048]{1,0:T(8,128)S(1)} %fusion.67, bf16[256,2048]{1,0:T(8,128)(2,1)} %all-gather.10.cloned.1.call-done, f32[256,256]{1,0:T(8,128)S(1)} %copy-done.1, f32[256,256]{1,0:T(8,128)S(1)} %reshape.160, f32[256,256]{1,0:T(8,128)S(1)} %copy-done.2, f32[256]{0:T(256)S(1)} %copy-done.13), kind=kOutput, calls=%fused_computation.87 | convolution fusion | flops 269746176 | bytes 4981760 | tf_op jit(solution)/shard_map/dot_general | solution.py:227
  213.9 9.5 %reduce-scatter.2.cloned.1.call-done = bf16[128,2048]{1,0:T(8,128)(2,1)} async-done(((bf16[256,2048]{1,0:T(8,128)(2,1)}), bf16[128,2048]{1,0:T(8,128)(2,1)}) %reduce-scatter.2.cloned.1.call-update) | async-done | bytes 524304 | tf_op jit(solution)/shard_map/reduce_scatter | solution.py:228
  (183 shorter events, 30.9 us)
Async XLA Ops:
  6.5 3.6 %copy-start.4 = (bf16[1,256,256]{2,1,0:T(8,128)(2,1)S(1)}, bf16[1,256,256]{2,1,0:T(8,128)(2,1)}, u32[]{:S(2)}) copy-start(bf16[1,256,256]{2,1,0:T(8,128)(2,1)} %param.29) | copy-start | bytes 393220
  6.5 202.9 %all-gather.8.cloned.1.call-start = ((), (), s32[]{:S(2)}) async-start(), calls=%async_computation.1 | async-start | bytes 1310720 | tf_op jit(solution)/shard_map/all_gather | solution.py:223
  7.3 4.0 %copy-start.3 = (f32[1,256,256]{2,1,0:T(8,128)S(1)}, f32[1,256,256]{2,1,0:T(8,128)}, u32[]{:S(2)}) copy-start(f32[1,256,256]{2,1,0:T(8,128)} %param.30) | copy-start | bytes 786436
  7.3 203.9 %all-gather.10.cloned.1.call-start = ((), (), s32[]{:S(2)}) async-start(), calls=%async_computation.2 | async-start | bytes 1310720 | tf_op jit(solution)/shard_map/all_gather | solution.py:224
  8.0 215.4 %reduce-scatter.2.cloned.1.call-start = ((), (), s32[]{:S(2)}) async-start(), calls=%async_computation.3 | async-start | bytes 1572864 | tf_op jit(solution)/shard_map/reduce_scatter | solution.py:228
  9.6 2.7 %copy-start.5 = (bf16[1,256,256]{2,1,0:T(8,128)(2,1)S(1)}, bf16[1,256,256]{2,1,0:T(8,128)(2,1)}, u32[]{:S(2)}) copy-start(bf16[1,256,256]{2,1,0:T(8,128)(2,1)} %param.28) | copy-start | bytes 393220
  9.7 2.9 %copy-start.6 = (bf16[1,256,256]{2,1,0:T(8,128)(2,1)S(1)}, bf16[1,256,256]{2,1,0:T(8,128)(2,1)}, u32[]{:S(2)}) copy-start(bf16[1,256,256]{2,1,0:T(8,128)(2,1)} %param.26) | copy-start | bytes 393220
  150.0 1.0 copy-start
  153.1 2.7 %copy-start.8 = (bf16[1,256,128]{2,1,0:T(8,128)(2,1)S(1)}, bf16[1,256,128]{2,1,0:T(8,128)(2,1)}, u32[]{:S(2)}) copy-start(bf16[1,256,128]{2,1,0:T(8,128)(2,1)} %param.22) | copy-start | bytes 196612
  153.1 2.8 %copy-start.9 = (bf16[1,256,128]{2,1,0:T(8,128)(2,1)S(1)}, bf16[1,256,128]{2,1,0:T(8,128)(2,1)}, u32[]{:S(2)}) copy-start(bf16[1,256,128]{2,1,0:T(8,128)(2,1)} %param.23) | copy-start | bytes 196612
  153.1 2.9 %copy-start.10 = (f32[1,256,4]{1,2,0:T(4,128)S(1)}, f32[1,256,4]{1,2,0:T(4,128)}, u32[]{:S(2)}) copy-start(f32[1,256,4]{1,2,0:T(4,128)} %param.24) | copy-start | bytes 12292
  153.4 44.3 %copy-start.7 = (bf16[1,256,256]{2,1,0:T(8,128)(2,1)S(1)}, bf16[1,256,256]{2,1,0:T(8,128)(2,1)}, u32[]{:S(2)}) copy-start(bf16[1,256,256]{2,1,0:T(8,128)(2,1)} %param.21) | copy-start | bytes 393220
  197.7 11.6 %copy-start.12 = (f32[256]{0:T(256)S(1)}, f32[256]{0:T(256)}, u32[]{:S(2)}) copy-start(f32[256]{0:T(256)} %param.25) | copy-start | bytes 3076
  197.7 0.8 copy-start.11
  208.2 3.0 %copy-start.1 = (f32[256,256]{1,0:T(8,128)S(1)}, f32[256,256]{1,0:T(8,128)}, u32[]{:S(2)}) copy-start(f32[256,256]{1,0:T(8,128)} %copy.73) | copy-start | bytes 786436
  208.2 3.0 %copy-start.2 = (f32[256,256]{1,0:T(8,128)S(1)}, f32[256,256]{1,0:T(8,128)}, u32[]{:S(2)}) copy-start(f32[256,256]{1,0:T(8,128)} %copy.72) | copy-start | bytes 786436
  208.2 3.0 %copy-start.13 = (f32[256]{0:T(256)S(1)}, f32[256]{0:T(256)}, u32[]{:S(2)}) copy-start(f32[256]{0:T(256)} %param.31) | copy-start | bytes 3076
Sparse Core Ops, SparseCore 0:
  9.2 29.8 all-gather.7
  40.9 27.0 all-gather.9
  214.0 9.3 reduce-scatter.1
where the time goes:
time: 231 us; the launch traced here: 230 us
  other arithmetic  85.3 us (37%)
  blocking collectives  71.9 us (31%)
  matrix products  30.9 us (13%)
  local copies, waits for them, and re-layouts  16.6 us (7%)
  between operations  13.5 us (6%)
  waiting for transfers between devices  11 us (5%)
    another operation x12, other arithmetic, one_span(): jax.scipy.linalg.solve_triangular(identity_span - mix_erase, right_side,...  79 us
    all_gather x2, blocking collectives, carried_in(): lax.all_gather(a.astype(kind), axis)  30.2 us
    dot_general x44, matrix products, product(): return jnp.einsum(form, left, right, precision=HIGHEST)  16.7 us
    all_gather x1, blocking collectives, forget_attention(): key_piece = lax.all_gather(key_rows, 'sp', axis=0, tiled=True)  14.5 us
    all_gather x1, blocking collectives, forget_attention(): value_piece = lax.all_gather(value_rows, 'sp', axis=0, tiled=True)  14 us
    all_gather x1, blocking collectives, forget_attention(): forget_all = lax.all_gather(forget_rows, 'sp', axis=0, tiled=True)  13.2 us
    reduce_scatter x1, waiting for transfers between devices, shards(): lax.psum_scatter(round_half(partial_value).astype(jnp.bfloat16), 'tp', sc...  9.53 us
    dynamic_slice x20, local copies, waits for them, and re-layouts, delta_attention(): lax.scan(one_span, start_state, (recept, key_float, value_float, unit_key...  7.59 us
  transfers between devices with their start and end apart: 3, of which 1 were waited for; matrix products, arithmetic and copies ran while one was open for 56% of the time, Pallas kernels for 0%

commit v1 on v0

--- a/solution.py
+++ b/solution.py
@@ -3,6 +3,7 @@
 import jax.numpy as jnp
 from jax import lax
 from jax.sharding import PartitionSpec as P
+from jax.lax import axis_index, axis_size, ppermute
 
 HEAD = 64
 SPAN = 64
@@ -51,7 +52,24 @@
         jnp.zeros((row_count, kv_count, group_size, HEAD), jnp.float32),
     )
     key_piece = lax.all_gather(key_rows, "sp", axis=0, tiled=True)
-    value_piece = lax.all_gather(value_rows, "sp", axis=0, tiled=True)
+
+    def compute_shards(x_local):
+        net_axis = "sp"
+        workers = axis_size(net_axis)
+        part_next = [(m - 1, m) for m in range(1, workers)] + [(workers - 1, 0)]
+        z1 = x_local
+        steps_seen = [z1]
+        for _ in [*range(workers - 1)]:
+            z1 = ppermute(z1, perm=part_next, axis_name=net_axis)
+            steps_seen += [z1]
+        heard = jnp.roll(
+            jnp.concatenate([*reversed(steps_seen)], axis=0),
+            (axis_index(net_axis) + 1) * z1.shape[0],
+            axis=0,
+        )
+        return heard
+
+    value_piece = compute_shards(value_rows)
     piece_rows = key_piece.shape[0]
     block_rows = math.gcd(piece_rows, 512)
 

time: 231 us -> 225 us (0.974)
  blocking collectives: 71.9 us -> 56.2 us
  starting transfers between devices: 0.08 us -> 4.86 us
  local copies, waits for them, and re-layouts: 16.6 us -> 20.6 us
  other arithmetic: 85.3 us -> 87.7 us
    all_gather x1 -> x0, blocking collectives: 14 us -> none  [forget_attention(): value_piece = lax.all_gather(value_rows, 'sp', axis=0, tiled=True)]
    ppermute x0 -> x3, starting transfers between devices: none -> 4.78 us  [compute_shards(): z1 = ppermute(z1, perm=part_next, axis_name=net_axis)]
    unnamed x28 -> x33, local copies, waits for them, and re-layouts: 1.29 us -> 3.84 us
  transfers between devices with their start and end apart: 3 -> 6, of which waited for: 1 -> 1; matrix products, arithmetic and copies ran while one was open for 56% -> 60% of each run, Pallas kernels for 0% -> 0%
where the time goes in v1:
time: 225 us; the launch traced here: 224 us
  other arithmetic  87.7 us (39%)
  blocking collectives  56.2 us (25%)
  matrix products  30.9 us (14%)
  local copies, waits for them, and re-layouts  20.6 us (9%)
  between operations  13.5 us (6%)
  waiting for transfers between devices  9.96 us (4%)
  starting transfers between devices  4.86 us (2%)
    another operation x12, other arithmetic, one_span(): jax.scipy.linalg.solve_triangular(identity_span - mix_erase, right_side,...  79 us
    all_gather x2, blocking collectives, carried_in(): lax.all_gather(a.astype(kind), axis)  27.9 us
    dot_general x44, matrix products, product(): return jnp.einsum(form, left, right, precision=HIGHEST)  16.7 us
    all_gather x1, blocking collectives, forget_attention(): forget_all = lax.all_gather(forget_rows, 'sp', axis=0, tiled=True)  14.3 us
    all_gather x1, blocking collectives, forget_attention(): key_piece = lax.all_gather(key_rows, 'sp', axis=0, tiled=True)  14 us
    reduce_scatter x1, waiting for transfers between devices, shards(): lax.psum_scatter(round_half(partial_value).astype(jnp.bfloat16), 'tp', sc...  9.17 us
    dynamic_slice x20, local copies, waits for them, and re-layouts, delta_attention(): lax.scan(one_span, start_state, (recept, key_float, value_float, unit_key...  7.59 us
    ppermute x3, starting transfers between devices, compute_shards(): z1 = ppermute(z1, perm=part_next, axis_name=net_axis)  4.78 us
  transfers between devices with their start and end apart: 6, of which 1 were waited for; matrix products, arithmetic and copies ran while one was open for 60% of the time, Pallas kernels for 0%

profile of v1, /device:TPU:0, one launch (start us, length us, event | category | flops | bytes accessed | tf_op | source)
XLA Modules:
  0.0 224.4 jit_solution(11633914125357268364)
XLA Ops:
  7.3 0.9 copy.56
  8.3 3.1 %collective-permute-start = (bf16[256,128]{0,1:T(8,128)(2,1)S(1)}, bf16[256,128]{0,1:T(8,128)(2,1)}, u32[]{:S(2)}, u32[]{:S(2)}) collective-permute-start(bf16[256,128]{0,1:T(8,128)(2,1)S(1)} %bitcast.239), channel_id=1, source_target_pairs={{0,8},{8,16},{16,24},{24,0},{1,9},{9,17},{17,25},{25,1},{2,10},{10... | collective-permute-start | bytes 196616 | tf_op jit(solution)/shard_map/ppermute | solution.py:63
  11.5 1.2 reshape.164
  13.6 1.0 reshape.163
  14.7 1.1 neg.24
  16.4 106.6 %while.56 = (s32[]{:T(128)}, f32[4,128,64]{1,2,0:T(8,128)S(1)}, f32[4,4,64,128]{3,2,1,0:T(8,128)}, f32[4,4,64,64]{3,1,2,0:T(4,128)}, f32[4,4,64,64]{3,1,2,0:T(4,...) while((s32[]{:T(128)}, f32[4,128,64]{1,2,0:T(8,128)S(1)}, ...), condition=%wide.region_10.11_spmd.clone.clone, body=%wide.region_8.10_spmd.clone.clone.sunk | while | flops 253308992 | bytes 5993869 | solution.py:193
  16.4 0.9 constant_dynamic-slice_fusion.21
  17.5 0.9 constant_dynamic-slice_fusion.20
  19.0 19.7 %custom-call.13 = f32[4,1,64,64]{2,3,1,0:T(8,128)S(1)} custom-call(f32[4,1,64,64]{3,2,1,0:T(8,128)S(1)} %fusion.172), custom_call_target="InvertDiagBlocksLowerTriangular" | custom-call | tf_op jit(solution)/shard_map/while/body/eval_jaxpr/jit(_solve_triangular)/vmap()/triangular_solve | solution.py:176
  43.0 0.9 constant_dynamic-slice_fusion.21
  45.6 19.7 %custom-call.13 = f32[4,1,64,64]{2,3,1,0:T(8,128)S(1)} custom-call(f32[4,1,64,64]{3,2,1,0:T(8,128)S(1)} %fusion.172), custom_call_target="InvertDiagBlocksLowerTriangular" | custom-call | tf_op jit(solution)/shard_map/while/body/eval_jaxpr/jit(_solve_triangular)/vmap()/triangular_solve | solution.py:176
  69.7 0.9 constant_dynamic-slice_fusion.21
  72.3 19.7 %custom-call.13 = f32[4,1,64,64]{2,3,1,0:T(8,128)S(1)} custom-call(f32[4,1,64,64]{3,2,1,0:T(8,128)S(1)} %fusion.172), custom_call_target="InvertDiagBlocksLowerTriangular" | custom-call | tf_op jit(solution)/shard_map/while/body/eval_jaxpr/jit(_solve_triangular)/vmap()/triangular_solve | solution.py:176
  98.9 19.7 %custom-call.13 = f32[4,1,64,64]{2,3,1,0:T(8,128)S(1)} custom-call(f32[4,1,64,64]{3,2,1,0:T(8,128)S(1)} %fusion.172), custom_call_target="InvertDiagBlocksLowerTriangular" | custom-call | tf_op jit(solution)/shard_map/while/body/eval_jaxpr/jit(_solve_triangular)/vmap()/triangular_solve | solution.py:176
  123.1 14.2 %all-gather.2 = bf16[16,64,64]{2,1,0:T(8,128)(2,1)S(1)} all-gather(bf16[4,64,64]{2,1,0:T(8,128)(2,1)S(1)} %get-tuple-element.682), channel_id=4, replica_groups=mesh['sp'=4,'fs'=4,'tp'=2] {'sp'}, dimensions={0}, use_global_device_ids=true | all-gather | bytes 163840 | tf_op jit(solution)/shard_map/all_gather | solution.py:17
  137.3 13.8 %all-gather.3 = bf16[16,64,64]{2,1,0:T(8,128)(2,1)S(1)} all-gather(bf16[4,64,64]{2,1,0:T(8,128)(2,1)S(1)} %get-tuple-element.681), channel_id=5, replica_groups=mesh['sp'=4,'fs'=4,'tp'=2] {'sp'}, dimensions={0}, use_global_device_ids=true | all-gather | bytes 163840 | tf_op jit(solution)/shard_map/all_gather | solution.py:17
  151.1 1.0 copy-done
  152.5 1.7 fusion.65
  156.5 14.3 %all-gather.1 = f32[1,1024,4]{1,2,0:T(4,128)} all-gather(f32[1,256,4]{1,2,0:T(4,128)S(1)} %copy-done.10), channel_id=3, replica_groups=mesh['sp'=4,'fs'=4,'tp'=2] {'sp'}, dimensions={1}, use_global_device_ids=true | all-gather | bytes 20480 | tf_op jit(solution)/shard_map/all_gather | solution.py:45
  170.8 1.4 collective-permute-start.2
  172.2 14.0 %all-gather = bf16[1,1024,128]{1,2,0:T(8,128)(2,1)S(1)} all-gather(bf16[1,256,128]{1,2,0:T(8,128)(2,1)S(1)} %copy.57), channel_id=2, replica_groups=mesh['sp'=4,'fs'=4,'tp'=2] {'sp'}, dimensions={1}, use_global_device_ids=true | all-gather | bytes 327680 | tf_op jit(solution)/shard_map/all_gather | solution.py:54
  188.0 14.4 %conditional.1 = (f32[256,2,2]{0,2,1:T(2,128)}, f32[256,2,2,64]{0,3,2,1:T(8,128)}) conditional(s32[]{:T(128)} %convert_element_type.58, () %tuple.52, (s32[]{:T(128)}, s32[]{:T(128)}, bf16[2048,128]{0,1:T(8,128)(2,1)S(1)}, s32[]{:T(128)}, s32[256]{0:T(256)S(1)}, /*index=5*/bf16[1,256,256]{2,1,0:T(8,128)(2,1)S(1)}, ...), branch_computations={%region_0.1_spmd, %region_1.6_spmd.clone} | conditional | flops 140318480 | bytes 9186850 | solution.py:119
  190.1 12.3 %while.54 = (s32[]{:T(128)}, f32[256,2,2]{0,2,1:T(2,128)S(1)}, f32[256,2,2]{0,2,1:T(2,128)}, f32[256,2,2,64]{0,3,2,1:T(8,128)}, s32[256]{0:T(256)}, /*index=5*/b...) while((s32[]{:T(128)}, f32[256,2,2]{0,2,1:T(2,128)S(1)}, ...), condition=%wide.wide.region_5.5_spmd.clone, body=%wide.wide.region_2.4_spmd.clone.sunk | while | flops 140318208 | bytes 8373459 | solution.py:114
  191.6 1.6 fusion.181
  194.2 1.2 fusion.185
  196.9 1.6 fusion.181
  198.9 1.3 fusion.184
  200.2 2.1 fusion.185
  202.4 1.0 multiply_reduce_fusion.2
  204.3 1.7 fusion.67
  206.0 2.7 %fusion.54 = bf16[256,2048]{1,0:T(8,128)(2,1)} fusion(f32[256,2048]{1,0:T(8,128)S(1)} %fusion.67, bf16[256,2048]{1,0:T(8,128)(2,1)} %all-gather.9.cloned.1.call-done, f32[256,256]{1,0:T(8,128)S(1)} %copy.74, f32[256,256]{1,0:T(8,128)S(1)} %reshape.160, f32[256,256]{1,0:T(8,128)S(1)} %copy-done.1, f32[256]{0:T(256)S(1)} %copy-done.12), kind=kOutput, calls=%fused_computation.88 | convolution fusion | flops 269746176 | bytes 4981760 | tf_op jit(solution)/shard_map/dot_general | solution.py:245
  208.7 9.2 %reduce-scatter.2.cloned.1.call-done = bf16[128,2048]{1,0:T(8,128)(2,1)} async-done(((bf16[256,2048]{1,0:T(8,128)(2,1)}), bf16[128,2048]{1,0:T(8,128)(2,1)}) %reduce-scatter.2.cloned.1.call-update) | async-done | bytes 524304 | tf_op jit(solution)/shard_map/reduce_scatter | solution.py:246
  (195 shorter events, 37.8 us)
Async XLA Ops:
  6.5 6.9 %copy-start.5 = (bf16[1,256,256]{2,1,0:T(8,128)(2,1)S(1)}, bf16[1,256,256]{2,1,0:T(8,128)(2,1)}, u32[]{:S(2)}) copy-start(bf16[1,256,256]{2,1,0:T(8,128)(2,1)} %param.29) | copy-start | bytes 393220
  6.5 197.7 %all-gather.7.cloned.1.call-start = ((), (), s32[]{:S(2)}) async-start(), calls=%async_computation.1 | async-start | bytes 1310720 | tf_op jit(solution)/shard_map/all_gather | solution.py:241
  7.3 198.7 %all-gather.9.cloned.1.call-start = ((), (), s32[]{:S(2)}) async-start(), calls=%async_computation.2 | async-start | bytes 1310720 | tf_op jit(solution)/shard_map/all_gather | solution.py:242
  8.2 6.4 %copy-start.2 = (bf16[1,256,128]{1,2,0:T(8,128)(2,1)}, bf16[1,256,128]{1,2,0:T(8,128)(2,1)S(1)}, u32[]{:S(2)}) copy-start(bf16[1,256,128]{1,2,0:T(8,128)(2,1)S(1)} %copy.56) | copy-start | bytes 196612
  8.3 6.4 %copy-start.4 = (f32[1,256,256]{2,1,0:T(8,128)S(1)}, f32[1,256,256]{2,1,0:T(8,128)}, u32[]{:S(2)}) copy-start(f32[1,256,256]{2,1,0:T(8,128)} %param.30) | copy-start | bytes 786436
  8.3 146.1 %collective-permute-start = (bf16[256,128]{0,1:T(8,128)(2,1)S(1)}, bf16[256,128]{0,1:T(8,128)(2,1)}, u32[]{:S(2)}, u32[]{:S(2)}) collective-permute-start(bf16[256,128]{0,1:T(8,128)(2,1)S(1)} %bitcast.239), channel_id=1, source_target_pairs={{0,8},{8,16},{16,24},{24,0},{1,9},{9,17},{17,25},{25,1},{2,10},{10... | collective-permute-start | bytes 196616 | tf_op jit(solution)/shard_map/ppermute | solution.py:63
  11.4 206.4 %reduce-scatter.2.cloned.1.call-start = ((), (), s32[]{:S(2)}) async-start(), calls=%async_computation.3 | async-start | bytes 1572864 | tf_op jit(solution)/shard_map/reduce_scatter | solution.py:246
  13.0 2.7 %copy-start.6 = (bf16[1,256,256]{2,1,0:T(8,128)(2,1)S(1)}, bf16[1,256,256]{2,1,0:T(8,128)(2,1)}, u32[]{:S(2)}) copy-start(bf16[1,256,256]{2,1,0:T(8,128)(2,1)} %param.28) | copy-start | bytes 393220
  13.0 2.9 %copy-start.7 = (bf16[1,256,256]{2,1,0:T(8,128)(2,1)S(1)}, bf16[1,256,256]{2,1,0:T(8,128)(2,1)}, u32[]{:S(2)}) copy-start(bf16[1,256,256]{2,1,0:T(8,128)(2,1)} %param.26) | copy-start | bytes 393220
  151.1 1.0 copy-start
  152.1 2.8 %copy-start.9 = (bf16[1,256,128]{2,1,0:T(8,128)(2,1)S(1)}, bf16[1,256,128]{2,1,0:T(8,128)(2,1)}, u32[]{:S(2)}) copy-start(bf16[1,256,128]{2,1,0:T(8,128)(2,1)} %param.22) | copy-start | bytes 196612
  154.2 2.3 %copy-start.10 = (f32[1,256,4]{1,2,0:T(4,128)S(1)}, f32[1,256,4]{1,2,0:T(4,128)}, u32[]{:S(2)}) copy-start(f32[1,256,4]{1,2,0:T(4,128)} %param.24) | copy-start | bytes 12292
  154.3 16.5 %collective-permute-start.1 = (bf16[256,128]{0,1:T(8,128)(2,1)}, bf16[256,128]{0,1:T(8,128)(2,1)S(1)}, u32[]{:S(2)}, u32[]{:S(2)}) collective-permute-start(bf16[256,128]{0,1:T(8,128)(2,1)} %collective-permute-done), channel_id=1, source_target_pairs={{0,8},{8,16},{16,24},{24,0},{1,9},{9,17},{17,25},{25,1},{2,10},{10... | collective-permute-start | bytes 196616 | tf_op jit(solution)/shard_map/ppermute | solution.py:63
  154.6 32.5 %copy-start.3 = (bf16[1,256,128]{1,2,0:T(8,128)(2,1)S(1)}, bf16[1,256,128]{1,2,0:T(8,128)(2,1)}, u32[]{:S(2)}) copy-start(bf16[1,256,128]{1,2,0:T(8,128)(2,1)} %copy-done.2) | copy-start | bytes 196612
  154.8 33.2 %copy-start.8 = (bf16[1,256,256]{2,1,0:T(8,128)(2,1)S(1)}, bf16[1,256,256]{2,1,0:T(8,128)(2,1)}, u32[]{:S(2)}) copy-start(bf16[1,256,256]{2,1,0:T(8,128)(2,1)} %param.21) | copy-start | bytes 393220
  170.8 15.4 %collective-permute-start.2 = (bf16[256,128]{0,1:T(8,128)(2,1)S(1)}, bf16[256,128]{0,1:T(8,128)(2,1)S(1)}, u32[]{:S(2)}, u32[]{:S(2)}) collective-permute-start(bf16[256,128]{0,1:T(8,128)(2,1)S(1)} %collective-permute-done.1), channel_id=1, source_target_pairs={{0,8},{8,16},{16,24},{24,0},{1,9},{9,17},{17,25},{25,1},{2,10},{10... | collective-permute-start | bytes 196616 | tf_op jit(solution)/shard_map/ppermute | solution.py:63
  188.0 2.1 copy-start.11
  202.4 3.6 %copy-start.1 = (f32[256,256]{1,0:T(8,128)S(1)}, f32[256,256]{1,0:T(8,128)}, u32[]{:S(2)}) copy-start(f32[256,256]{1,0:T(8,128)} %copy.73) | copy-start | bytes 786436
  202.4 3.6 %copy-start.12 = (f32[256]{0:T(256)S(1)}, f32[256]{0:T(256)}, u32[]{:S(2)}) copy-start(f32[256]{0:T(256)} %param.31) | copy-start | bytes 3076
Sparse Core Ops, SparseCore 0:
  9.2 30.1 all-gather.6
  41.1 26.5 all-gather.8
  208.8 8.9 reduce-scatter.1
